TPU v7x, 32 devices: a whole 2x2x4 slice. The times are simulated.
32 devices in a mesh: vp: 4 (over y, x), dp: 8 (over z, core).
Axes of the slice: x: 2, y: 2, z: 4, core: 2. Of those that a mesh axis runs over, the one named last changes fastest.
Arguments:
- hidden_act: bfloat16 [4096, 8192], P('dp', 'vp'), may hold values from 0 to 36
- down_weight: bfloat16 [8192, 2048], P('vp'), may hold values from -0.0625 to 0.0625
- residual: bfloat16 [4096, 2048], P(('dp', 'vp')), may hold values from -300 to 300
- post_gain: float32 [2048], replicated, may hold values from 0.1 to 1.9
- final_gain: float32 [2048], replicated, may hold values from 0.1 to 1.9
- vocab: bfloat16 [2048, 32768], P(None, 'vp'), may hold values from -0.33 to 0.33
- vocab_bias: float32 [32768], P('vp'), may hold values from -2.5 to 2.5
- target_ids: int32 [4096, 4], P('dp'), may hold values from 0 to 32767
- target_weights: float32 [4096, 4], P('dp'), may hold values from 0 to 1, as said below
Outputs:
- losses: float32 [4096], P(('dp', 'vp'))
- stream_grad: float32 [4096, 2048], P(('dp', 'vp'))
- vocab_grad: float32 [2048, 32768], P('dp', 'vp')
Inputs may be any that keep to these rules, and one draw needn't show every extreme that they name: `target_weights`: the 4 weights of a token add up to one.
All inputs are finite; a program needn't handle non-finite values.
Results may differ from a plain program's by a relative error of at most 0.01225.
Values may be sent and summed in bfloat16 or wider, within the bound.
A program may use at most 192 MiB of HBM per device.

v0:
```python
import jax
import jax.numpy as jnp
from jax import lax
from jax.sharding import PartitionSpec as P

COL_BLOCK = 512


epsilon = 1e-06
z_weight = 0.001
loss_scale = 32.0


def inverse_rms(values):
    return lax.rsqrt(jnp.mean(values * values, axis=-1, keepdims=True) + epsilon)


def shards(
    hidden_act,
    down_weight,
    residual,
    post_gain,
    final_gain,
    vocab,
    vocab_bias,
    target_ids,
    target_weights,
):
    own_rows = residual.shape[0]
    group_rows = hidden_act.shape[0]
    width = vocab.shape[0]
    columns = vocab.shape[1]
    blocks = columns // COL_BLOCK
    vp_index = lax.axis_index("vp")
    branch = lax.psum_scatter(
        jnp.dot(hidden_act, down_weight, preferred_element_type=jnp.float32),
        "vp",
        scatter_dimension=0,
        tiled=True,
    )
    stream = residual.astype(jnp.float32) + branch * inverse_rms(branch) * post_gain
    inverse = inverse_rms(stream)
    normed = (stream * inverse * final_gain).astype(jnp.bfloat16)
    gathered = lax.all_gather(normed, "vp", axis=0, tiled=True)
    local_ids = target_ids - vp_index * columns
    vocab_split = vocab.reshape(width, blocks, COL_BLOCK)
    bias_split = vocab_bias.reshape(blocks, COL_BLOCK)

    def block_wanted(block_index):
        position = block_index * COL_BLOCK + lax.broadcasted_iota(jnp.int32, (1, COL_BLOCK), 1)
        wanted = jnp.zeros((group_rows, COL_BLOCK), jnp.float32)
        for target_k in range(target_ids.shape[1]):
            wanted = wanted + jnp.where(
                local_ids[:, target_k : target_k + 1] == position,
                target_weights[:, target_k : target_k + 1],
                0.0,
            )
        return wanted

    def gather_stats(running, block_index):
        run_max, run_sum, run_target = running
        weight_block = lax.dynamic_index_in_dim(vocab_split, block_index, 1, keepdims=False)
        bias_block = lax.dynamic_index_in_dim(bias_split, block_index, 0, keepdims=False)
        scores = jnp.dot(gathered, weight_block, preferred_element_type=jnp.float32) + bias_block
        wanted = block_wanted(block_index)
        new_max = jnp.maximum(run_max, jnp.max(scores, axis=1))
        run_sum = run_sum * jnp.exp(run_max - new_max) + jnp.sum(
            jnp.exp(scores - new_max[:, None]), axis=1
        )
        run_target = run_target + jnp.sum(wanted * scores, axis=1)
        return ((new_max, run_sum, run_target), scores)

    zeros_rows = jnp.zeros((group_rows,), jnp.float32)
    start_stats = (jnp.full((group_rows,), -jnp.inf, jnp.float32), zeros_rows, zeros_rows)
    local_stats, stored_scores = lax.scan(gather_stats, start_stats, jnp.arange(blocks))
    local_max, local_sum, local_target = local_stats
    row_max = lax.pmax(local_max, "vp")
    row_sum, target_score = lax.psum((local_sum * jnp.exp(local_max - row_max), local_target), "vp")
    log_norm = row_max + jnp.log(row_sum)
    group_losses = log_norm - target_score + z_weight * log_norm * log_norm
    losses = lax.dynamic_slice_in_dim(group_losses, vp_index * own_rows, own_rows, 0)
    factor = (1.0 + 2.0 * z_weight * log_norm)[:, None]

    def score_grad(inputs):
        block_index, scores = inputs
        probability = jnp.exp(scores - log_norm[:, None])
        return (loss_scale * (probability * factor - block_wanted(block_index))).astype(
            jnp.bfloat16
        )

    score_grads = lax.map(score_grad, (jnp.arange(blocks), stored_scores))
    row_grad = lax.psum_scatter(
        jnp.einsum("jrc,djc->rd", score_grads, vocab_split, preferred_element_type=jnp.float32),
        "vp",
        scatter_dimension=0,
        tiled=True,
    )
    slice_width = width // lax.axis_size("dp")
    vocab_grad = lax.psum_scatter(
        jnp.einsum("rd,jrc->djc", gathered, score_grads, preferred_element_type=jnp.float32)
        .reshape(lax.axis_size("dp") * slice_width, columns)
        .astype(jnp.bfloat16),
        "dp",
        scatter_dimension=0,
        tiled=True,
    ).astype(jnp.float32)
    upstream = row_grad * final_gain
    stream_grad = inverse * (
        upstream - stream * inverse * inverse * jnp.mean(upstream * stream, axis=-1, keepdims=True)
    )
    return (losses, stream_grad, vocab_grad)


def solution(mesh):
    in_specs = (
        P("dp", "vp"),
        P("vp", None),
        P(("dp", "vp"), None),
        P(),
        P(),
        P(None, "vp"),
        P("vp"),
        P("dp", None),
        P("dp", None),
    )
    out_specs = (P(("dp", "vp")), P(("dp", "vp"), None), P("dp", "vp"))
    return jax.shard_map(shards, mesh=mesh, in_specs=in_specs, out_specs=out_specs, check_vma=False)
```

profile of v0, /device:TPU:0, one launch (start us, length us, event | category | flops | bytes accessed | tf_op | source)
XLA Modules:
  0.0 779.3 jit_solution(12714494460558069594)
XLA Ops:
  8.8 9.4 %fusion.19 = f32[512,2048]{1,0:T(8,128)} fusion(bf16[512,2048]{1,0:T(8,128)(2,1)S(1)} %copy-done, bf16[2048,2048]{1,0:T(8,128)(2,1)} %param.14), kind=kOutput, calls=%fused_computation.44 | convolution fusion | flops 4294967296 | bytes 14680064 | tf_op jit(solution)/shard_map/dot_general | solution.py:36
  18.2 55.4 %reduce-scatter.4.cloned.1.call-done = f32[128,2048]{1,0:T(8,128)} async-done(((f32[512,2048]{1,0:T(8,128)}), f32[128,2048]{1,0:T(8,128)}) %reduce-scatter.4.cloned.1.call-update) | async-done | bytes 1048592 | tf_op jit(solution)/shard_map/reduce_scatter | solution.py:35
  75.0 1.6 multiply_reduce_fusion.1
  76.6 2.3 multiply_convert_fusion.1
  79.1 44.5 %copy.19 = bf16[2048,8192]{0,1:T(8,128)(2,1)} copy(bf16[2048,8192]{1,0:T(8,128)(2,1)} %param.18) | data formatting | bytes 67108864 | tf_op args[5]
  123.7 136.4 %while.28 = (s32[]{:T(128)}, f32[512]{0:T(512)S(1)}, f32[512]{0:T(512)S(1)}, f32[512]{0:T(512)S(1)}, f32[16,512,512]{1,2,0:T(8,128)}, /*index=5*/s32[16]{0:T(128...) while((s32[]{:T(128)}, f32[512]{0:T(512)S(1)}, ...), condition=%wide.region_7.8_spmd.clone, body=%wide.region_3.7_spmd.clone.sunk | while | flops 1078201856 | bytes 8483050 | solution.py:75
  126.3 3.5 fusion.38
  134.8 3.5 fusion.38
  143.3 3.5 fusion.38
  151.9 3.5 fusion.38
  160.4 3.5 fusion.38
  168.9 3.5 fusion.38
  177.4 3.5 fusion.38
  185.9 3.5 fusion.38
  194.5 3.5 fusion.38
  203.0 3.5 fusion.38
  211.5 3.5 fusion.38
  220.1 3.5 fusion.38
  228.6 3.5 fusion.38
  237.1 3.5 fusion.38
  245.6 3.5 fusion.38
  254.2 3.5 fusion.38
  260.2 7.4 pmax.7
  267.6 9.5 %all-reduce = (f32[512]{0:T(512)S(1)}, f32[512]{0:T(512)S(1)}) all-reduce(f32[512]{0:T(512)S(1)} %exponential_multiply_fusion, f32[512]{0:T(512)S(1)} %get-tuple-element.107), channel_id=1, replica_groups=mesh['vp'=4,'dp'=8] {'vp'}, use_global_device_ids=true, to_apply=%region_9.10 | all-reduce | flops 1024 | bytes 8192 | tf_op jit(solution)/shard_map/psum | solution.py:78
  277.1 72.5 %while.27 = (s32[]{:T(128)}, bf16[16,512,512]{2,1,0:T(8,128)(2,1)}, f32[16,512,512]{1,2,0:T(8,128)}, f32[512]{0:T(512)S(1)}, f32[512,1]{0,1:T(1,128)S(1)}, /*ind...) while((s32[]{:T(128)}, bf16[16,512,512]{2,1,0:T(8,128)(2,1)}, ...), condition=%wide.region_12.13_spmd, body=%wide.region_11.12_spmd.sunk | while | flops 4194819 | bytes 5824657 | solution.py:91
  280.0 1.6 fusion.36
  284.6 1.6 fusion.36
  289.1 1.6 fusion.36
  293.6 1.6 fusion.36
  298.1 1.6 fusion.36
  302.7 1.6 fusion.36
  307.2 1.6 fusion.36
  311.7 1.6 fusion.36
  316.3 1.6 fusion.36
  320.8 1.6 fusion.36
  325.3 1.6 fusion.36
  329.9 1.6 fusion.36
  334.4 1.6 fusion.36
  338.9 1.6 fusion.36
  343.4 1.6 fusion.36
  348.0 1.6 fusion.36
  349.6 25.0 %convolution_bitcast_fusion = f32[512,2048]{1,0:T(8,128)} fusion(bf16[16,512,512]{2,1,0:T(8,128)(2,1)} %get-tuple-element.109, bf16[2048,16,512]{0,2,1:T(8,128)(2,1)} %get-tuple-element.486), kind=kOutput, calls=%fused_computation.22 | convolution fusion | flops 17179869184 | bytes 46137344 | tf_op jit(solution)/shard_map/jrc,djc->rd/dot_general | solution.py:93
  374.8 24.9 %convolution_convert_fusion = bf16[2048,16,512]{0,2,1:T(8,128)(2,1)} fusion(bf16[16,512,512]{2,1,0:T(8,128)(2,1)} %get-tuple-element.109, bf16[512,2048]{1,0:T(8,128)(2,1)S(1)} %copy-done.9), kind=kOutput, calls=%fused_computation.21 | convolution fusion | flops 17196646400 | bytes 44040192 | tf_op jit(solution)/shard_map/rd,jrc->djc/dot_general | solution.py:100
  399.7 40.4 %copy.24 = bf16[2048,8192]{1,0:T(8,128)(2,1)} copy(bf16[2048,8192]{0,1:T(8,128)(2,1)} %bitcast.103) | data formatting | bytes 67108864 | tf_op jit(solution)/shard_map/convert_element_type | solution.py:102
  441.3 1.9 multiply_reduce_fusion
  443.2 2.8 subtract_multiply_fusion
  446.0 320.2 %reduce-scatter.8.cloned.1.call-done = bf16[256,8192]{1,0:T(8,128)(2,1)} async-done(((bf16[2048,8192]{1,0:T(8,128)(2,1)}), bf16[256,8192]{1,0:T(8,128)(2,1)}) %reduce-scatter.8.cloned.1.call-update) | async-done | bytes 4194320 | tf_op jit(solution)/shard_map/reduce_scatter | solution.py:99
  766.2 6.6 convert_element_type.23
  (303 shorter events, 78.1 us)
Async XLA Ops:
  7.2 1.6 copy-start
  7.2 67.8 %copy-start.5 = (f32[2048]{0:T(1024)S(1)}, f32[2048]{0:T(1024)}, u32[]{:S(2)}) copy-start(f32[2048]{0:T(1024)} %param.16) | copy-start | bytes 24580
  7.2 67.8 %copy-start.3 = (bf16[128,2048]{1,0:T(8,128)(2,1)S(1)}, bf16[128,2048]{1,0:T(8,128)(2,1)}, u32[]{:S(2)}) copy-start(bf16[128,2048]{1,0:T(8,128)(2,1)} %param.15) | copy-start | bytes 1572868
  7.2 69.4 %copy-start.6 = (f32[2048]{0:T(1024)S(1)}, f32[2048]{0:T(1024)}, u32[]{:S(2)}) copy-start(f32[2048]{0:T(1024)} %param.17) | copy-start | bytes 24580
  7.2 66.4 %reduce-scatter.4.cloned.1.call-start = ((), (), s32[]{:S(2)}) async-start(), calls=%async_computation.3 | async-start | bytes 5242880 | tf_op jit(solution)/shard_map/reduce_scatter | solution.py:35
  18.2 105.5 %all-gather.2.cloned.1.call-start = ((), (), s32[]{:S(2)}) async-start(), calls=%async_computation.4 | async-start | bytes 2621440 | tf_op jit(solution)/shard_map/all_gather | solution.py:44
  79.0 361.7 %reduce-scatter.6.cloned.1.call-start = ((), (), s32[]{:S(2)}) async-start(), calls=%async_computation.5 | async-start | bytes 5242880 | tf_op jit(solution)/shard_map/reduce_scatter | solution.py:92
  79.1 44.5 %copy-start.7 = (f32[8192]{0:T(1024)S(1)}, f32[8192]{0:T(1024)}, u32[]{:S(2)}) copy-start(f32[8192]{0:T(1024)} %param.19) | copy-start | bytes 98308
  79.1 44.5 %copy-start.8 = (s32[512,4]{0,1:T(4,128)S(1)}, s32[512,4]{0,1:T(4,128)}, u32[]{:S(2)}) copy-start(s32[512,4]{0,1:T(4,128)} %param.20) | copy-start | bytes 24580
  79.1 44.6 %copy-start.4 = (f32[512,4]{0,1:T(4,128)S(1)}, f32[512,4]{0,1:T(4,128)}, u32[]{:S(2)}) copy-start(f32[512,4]{0,1:T(4,128)} %param.21) | copy-start | bytes 24580
  349.6 25.2 %copy-start.9 = (bf16[512,2048]{1,0:T(8,128)(2,1)S(1)}, bf16[512,2048]{1,0:T(8,128)(2,1)}, u32[]{:S(2)}) copy-start(bf16[512,2048]{1,0:T(8,128)(2,1)} %get-tuple-element.500) | copy-start | bytes 6291460
  374.6 391.6 %reduce-scatter.8.cloned.1.call-start = ((), (), s32[]{:S(2)}) async-start(), calls=%async_computation.6 | async-start | bytes 37748736 | tf_op jit(solution)/shard_map/reduce_scatter | solution.py:99
  440.1 1.2 copy-start.2
  441.3 331.4 %copy-start.1 = (bf16[512,2048]{1,0:T(8,128)(2,1)S(1)}, bf16[512,2048]{1,0:T(8,128)(2,1)}, u32[]{:S(2)}) copy-start(bf16[512,2048]{1,0:T(8,128)(2,1)} %param.13) | copy-start | bytes 6291460
Sparse Core Ops, SparseCore 0:
  18.3 55.3 reduce-scatter.3
  79.1 35.1 all-gather.1
  374.7 52.5 reduce-scatter.5
  440.2 325.8 reduce-scatter.7
where the time goes:
time: 783 us; the launch traced here: 779 us
  waiting for transfers between devices  376 us (48%)
  local copies, waits for them, and re-layouts  150 us (19%)
  matrix products  116 us (15%)
  loops' own time  53.4 us (7%)
  other arithmetic  53.3 us (7%)
  blocking collectives  16.9 us (2%)
  between operations  14 us (2%)
    reduce_scatter x1, waiting for transfers between devices, shards(): lax.psum_scatter(jnp.einsum('rd,jrc->djc', gathered, score_grads, preferr...  320 us
    dot_general x16, matrix products, gather_stats(): jnp.dot(gathered, weight_block, preferred_element_type=jnp.float32)  56.3 us
    reduce_scatter x1, waiting for transfers between devices, shards(): lax.psum_scatter(jnp.dot(hidden_act, down_weight, preferred_element_type=...  55.4 us
    unnamed x21, local copies, waits for them, and re-layouts  46.7 us
    another operation x1, loops' own time, shards(): lax.scan(gather_stats, start_stats, jnp.arange(blocks))  42.4 us
    convert_element_type x1, local copies, waits for them, and re-layouts, shards(): vocab_grad = lax.psum_scatter(jnp.einsum('rd,jrc->djc', gathered, score_g...  40.4 us
    dynamic_slice x32, local copies, waits for them, and re-layouts, shards(): score_grads = lax.map(score_grad, (jnp.arange(blocks), stored_scores))  26 us
    dynamic_update_slice x16, other arithmetic, shards(): score_grads = lax.map(score_grad, (jnp.arange(blocks), stored_scores))  25.7 us
  transfers between devices with their start and end apart: 4, of which 2 were waited for; matrix products, arithmetic and copies ran while one was open for 15% of the time, Pallas kernels for 0%

commit v1 on v0

v1 whole, which is shorter than its diff:
```python
import jax
import jax.numpy as jnp
from jax import lax
from jax.sharding import PartitionSpec as P

CHUNKS = 4


epsilon = 1e-06
z_weight = 0.001
loss_scale = 32.0


def inverse_rms(values):
    return lax.rsqrt(jnp.mean(values * values, axis=-1, keepdims=True) + epsilon)


def shards(
    hidden_act,
    down_weight,
    residual,
    post_gain,
    final_gain,
    vocab,
    vocab_bias,
    target_ids,
    target_weights,
):
    own_rows = residual.shape[0]
    group_rows = hidden_act.shape[0]
    columns = vocab.shape[1]
    vp_index = lax.axis_index("vp")
    branch = lax.psum_scatter(
        jnp.dot(hidden_act, down_weight, preferred_element_type=jnp.float32),
        "vp",
        scatter_dimension=0,
        tiled=True,
    )
    stream = residual.astype(jnp.float32) + branch * inverse_rms(branch) * post_gain
    inverse = inverse_rms(stream)
    normed = (stream * inverse * final_gain).astype(jnp.bfloat16)
    gathered = lax.all_gather(normed, "vp", axis=0, tiled=True)
    local_ids = target_ids - vp_index * columns
    position = lax.broadcasted_iota(jnp.int32, (1, columns), 1)
    wanted = jnp.zeros((group_rows, columns), jnp.float32)
    for target_k in range(target_ids.shape[1]):
        wanted = wanted + jnp.where(
            local_ids[:, target_k : target_k + 1] == position,
            target_weights[:, target_k : target_k + 1],
            0.0,
        )
    scores = jnp.dot(gathered, vocab, preferred_element_type=jnp.float32) + vocab_bias[None, :]
    local_max = jnp.max(scores, axis=1)
    local_sum = jnp.sum(jnp.exp(scores - local_max[:, None]), axis=1)
    local_target = jnp.sum(wanted * scores, axis=1)
    stats = lax.all_gather(jnp.stack([local_max, local_sum, local_target]), "vp", axis=0)
    row_max = jnp.max(stats[:, 0], axis=0)
    row_sum = jnp.sum(stats[:, 1] * jnp.exp(stats[:, 0] - row_max), axis=0)
    target_score = jnp.sum(stats[:, 2], axis=0)
    log_norm = row_max + jnp.log(row_sum)
    group_losses = log_norm - target_score + z_weight * log_norm * log_norm
    losses = lax.dynamic_slice_in_dim(group_losses, vp_index * own_rows, own_rows, 0)
    factor = (1.0 + 2.0 * z_weight * log_norm)[:, None]
    probability = jnp.exp(scores - log_norm[:, None])
    score_grads = (loss_scale * (probability * factor - wanted)).astype(jnp.bfloat16)
    chunk = columns // CHUNKS
    pieces = []
    for index in range(CHUNKS):
        part = score_grads[:, index * chunk : (index + 1) * chunk]
        grad = lax.dot_general(
            gathered, part, (((0,), (0,)), ((), ())), preferred_element_type=jnp.float32
        ).astype(jnp.bfloat16)
        pieces.append(lax.psum_scatter(grad, "dp", scatter_dimension=0, tiled=True))
    row_grad = lax.psum_scatter(
        lax.dot_general(
            score_grads, vocab, (((1,), (1,)), ((), ())), preferred_element_type=jnp.float32
        ),
        "vp",
        scatter_dimension=0,
        tiled=True,
    )
    vocab_grad = jnp.concatenate([piece.astype(jnp.float32) for piece in pieces], axis=1)
    upstream = row_grad * final_gain
    stream_grad = inverse * (
        upstream - stream * inverse * inverse * jnp.mean(upstream * stream, axis=-1, keepdims=True)
    )
    return (losses, stream_grad, vocab_grad)


def solution(mesh):
    in_specs = (
        P("dp", "vp"),
        P("vp", None),
        P(("dp", "vp"), None),
        P(),
        P(),
        P(None, "vp"),
        P("vp"),
        P("dp", None),
        P("dp", None),
    )
    out_specs = (P(("dp", "vp")), P(("dp", "vp"), None), P("dp", "vp"))
    return jax.shard_map(shards, mesh=mesh, in_specs=in_specs, out_specs=out_specs, check_vma=False)
```

time: 783 us -> 640 us (0.82)
  local copies, waits for them, and re-layouts: 150 us -> 2.16 us
  waiting for transfers between devices: 376 us -> 459 us
  loops' own time: 53.4 us -> 0 us
  matrix products: 116 us -> 102 us
  blocking collectives: 16.9 us -> 8.32 us
    another operation x2 -> x0, loops' own time: 53.4 us -> none  [the longest x1 42.4 us: shards(): lax.scan(gather_stats, start_stats, jnp.arange(blocks))]
    reduce_scatter x2 -> x5, waiting for transfers between devices: 320 us -> 369 us  [the longest x4 358 us: shards(): pieces.append(lax.psum_scatter(grad, 'dp', scatter_dimension=0, tiled=True))]
    unnamed x21 -> x20, local copies, waits for them, and re-layouts: 46.7 us -> 1.55 us
    dynamic_slice x80 -> x0, local copies, waits for them, and re-layouts: 44.9 us -> none  [the longest x32 26 us: shards(): score_grads = lax.map(score_grad, (jnp.arange(blocks), stored_scores))]
    convert_element_type x1 -> x0, local copies, waits for them, and re-layouts: 40.4 us -> none  [shards(): vocab_grad = lax.psum_scatter(jnp.einsum('rd,jrc->djc', gathered, score_g...]
    all_gather x1, waiting for transfers between devices: 0.02 us -> 34.7 us  [shards(): gathered = lax.all_gather(normed, 'vp', axis=0, tiled=True)]
    dynamic_update_slice x16 -> x0, other arithmetic: 25.7 us -> none  [shards(): score_grads = lax.map(score_grad, (jnp.arange(blocks), stored_scores))]
    dynamic_update_slice x16 -> x0, local copies, waits for them, and re-layouts: 17 us -> none  [shards(): lax.scan(gather_stats, start_stats, jnp.arange(blocks))]
  transfers between devices with their start and end apart: 4 -> 7, of which waited for: 2 -> 7; matrix products, arithmetic and copies ran while one was open for 15% -> 7% of each run, Pallas kernels for 0% -> 0%
where the time goes in v1:
time: 640 us; the launch traced here: 637 us
  waiting for transfers between devices  459 us (72%)
  matrix products  102 us (16%)
  other arithmetic  50.3 us (8%)
  between operations  14.5 us (2%)
  blocking collectives  8.32 us (1%)
    reduce_scatter x4, waiting for transfers between devices, shards(): pieces.append(lax.psum_scatter(grad, 'dp', scatter_dimension=0, tiled=True))  358 us
    reduce_scatter x1, waiting for transfers between devices, shards(): lax.psum_scatter(jnp.dot(hidden_act, down_weight, preferred_element_type=...  55.4 us
    dot_general x4, matrix products, shards(): lax.dot_general(gathered, part, (((0,), (0,)), ((), ())), preferred_eleme...  40.4 us
    all_gather x1, waiting for transfers between devices, shards(): gathered = lax.all_gather(normed, 'vp', axis=0, tiled=True)  34.7 us
    dot_general x1, matrix products, shards(): jnp.dot(gathered, vocab, preferred_element_type=jnp.float32)  27.3 us
    dot_general x1, matrix products, shards(): lax.dot_general(score_grads, vocab, (((1,), (1,)), ((), ())), preferred_e...  24.9 us
    convert_element_type x1, other arithmetic, shards(): (loss_scale * (probability * factor - wanted)).astype(jnp.bfloat16)  18.7 us
    reduce_sum x1, other arithmetic, shards(): local_sum = jnp.sum(jnp.exp(scores - local_max[:, None]), axis=1)  16.2 us
  transfers between devices with their start and end apart: 7, of which 7 were waited for; matrix products, arithmetic and copies ran while one was open for 7% of the time, Pallas kernels for 0%

profile of v1, /device:TPU:0, one launch (start us, length us, event | category | flops | bytes accessed | tf_op | source)
XLA Modules:
  0.0 637.4 jit_solution(9418689511885468283)
XLA Ops:
  7.2 0.0 copy-start
  7.2 0.0 copy-start.6
  7.2 0.0 copy-start.4
  7.2 0.0 reduce-scatter.7.cloned.1.call-start
  7.3 1.5 copy-done
  8.8 9.4 %fusion.12 = f32[512,2048]{1,0:T(8,128)} fusion(bf16[512,2048]{1,0:T(8,128)(2,1)S(1)} %copy-done, bf16[2048,2048]{1,0:T(8,128)(2,1)} %param.10), kind=kOutput, calls=%fused_computation.43 | convolution fusion | flops 4294967296 | bytes 14680064 | tf_op jit(solution)/shard_map/dot_general | solution.py:34
  18.1 0.0 reduce-scatter.7.cloned.1.call-update
  18.2 0.0 all-gather.4.cloned.1.call-start
  18.2 55.4 %reduce-scatter.7.cloned.1.call-done = f32[128,2048]{1,0:T(8,128)} async-done(((f32[512,2048]{1,0:T(8,128)}), f32[128,2048]{1,0:T(8,128)}) %reduce-scatter.7.cloned.1.call-update) | async-done | bytes 1048592 | tf_op jit(solution)/shard_map/reduce_scatter | solution.py:33
  73.6 1.4 multiply_reduce_fusion.3
  75.0 1.6 multiply_reduce_fusion.2
  76.6 0.0 copy-done.7
  76.6 2.3 multiply_convert_fusion.1
  79.0 0.0 all-gather.4.cloned.1.call-update
  79.0 0.6 reduce-scatter.9.cloned.1.call-start
  79.6 0.0 copy-done.8
  79.6 0.0 copy-done.9
  79.6 34.7 %all-gather.4.cloned.1.call-done = bf16[512,2048]{1,0:T(8,128)(2,1)} async-done(((bf16[128,2048]{1,0:T(8,128)(2,1)}), bf16[512,2048]{1,0:T(8,128)(2,1)}) %all-gather.4.cloned.1.call-update) | async-done | bytes 2097168 | tf_op jit(solution)/shard_map/all_gather | solution.py:42
  114.3 0.0 copy-done.5
  114.3 27.3 %add_reduce_fusion = (f32[512]{0:T(512)S(1)}, f32[512,8192]{1,0:T(8,128)}) fusion(f32[8192]{0:T(1024)S(1)} %copy-done.5, bf16[512,2048]{1,0:T(8,128)(2,1)} %all-gather.4.cloned.1.call-done, bf16[2048,8192]{1,0:T(8,128)(2,1)} %param.14), kind=kOutput, calls=%fused_computation.8 | convolution fusion | flops 17188257792 | bytes 52463616 | tf_op jit(solution)/shard_map/dot_general | solution.py:52
  141.6 16.2 %exponential_reduce_fusion = (f32[512]{0:T(512)S(1)}, f32[512]{0:T(512)S(1)}) fusion(f32[512,8192]{1,0:T(8,128)} %get-tuple-element.22, f32[512]{0:T(512)S(1)} %get-tuple-element.21, f32[8192]{0:T(1024)S(1)} %copy-done.5, f32[512]{0:T(512)S(1)} %bitcast.39, s32[512]{0:T(512)S(1)} %bitcast.45, f32[512]{0:T(512)S(1)} %bitcast.41, s32[512]{0:T(512)S(1)} %bitcast.47, ...), kind=kLoop, calls=%fused_computation.7 | loop fusion | flops 67107840 | bytes 16832512 | tf_op jit(solution)/shard_map/reduce_sum | solution.py:54
  157.8 8.3 %all-gather.1 = f32[4,3,512]{2,1,0:T(4,128)S(1)} all-gather(f32[1,3,512]{2,1,0:T(4,128)S(1)} %maximum_bitcast_fusion), channel_id=2, replica_groups=mesh['vp'=4,'dp'=8] {'vp'}, dimensions={0}, use_global_device_ids=true | all-gather | bytes 30720 | tf_op jit(solution)/shard_map/all_gather | solution.py:56
  166.2 0.0 copy-done.2
  166.3 18.7 %multiply_convert_fusion = bf16[512,8192]{1,0:T(8,128)(2,1)} fusion(f32[512,8192]{1,0:T(8,128)S(1)} %copy-done.2, f32[512]{0:T(512)S(1)} %get-tuple-element.7, f32[512]{0:T(512)S(1)} %get-tuple-element.8, f32[512]{0:T(512)S(1)} %bitcast.40, s32[512]{0:T(512)S(1)} %bitcast.46, f32[512]{0:T(512)S(1)} %bitcast.42, s32[512]{0:T(512)S(1)} %bitcast.48, ...), kind=kLoop, calls=%fused_computation | loop fusion | flops 71303168 | bytes 25219072 | tf_op jit(solution)/shard_map/convert_element_type | solution.py:65
  184.9 24.9 %fusion.13 = f32[512,2048]{1,0:T(8,128)} fusion(bf16[512,8192]{1,0:T(8,128)(2,1)} %multiply_convert_fusion, bf16[2048,8192]{1,0:T(8,128)(2,1)} %param.14), kind=kOutput, calls=%fused_computation.44 | convolution fusion | flops 17179869184 | bytes 46137344 | tf_op jit(solution)/shard_map/dot_general | solution.py:75
  209.9 0.0 reduce-scatter.9.cloned.1.call-update
  209.9 0.3 reduce-scatter.17.cloned.1.call-start
  210.1 10.0 %convolution_convert_fusion = bf16[2048,2048]{1,0:T(8,128)(2,1)} fusion(bf16[512,2048]{1,0:T(8,128)(2,1)} %all-gather.4.cloned.1.call-done, bf16[512,8192]{1,0:T(8,128)(2,1)} %multiply_convert_fusion), kind=kOutput, calls=%fused_computation.9 | convolution fusion | flops 4299161600 | bytes 12582912 | tf_op jit(solution)/shard_map/dot_general | solution.py:70
  220.2 0.0 reduce-scatter.17.cloned.1.call-update
  220.2 0.0 reduce-scatter.15.cloned.1.call-start
  220.2 10.0 %convolution_convert_fusion.1 = bf16[2048,2048]{1,0:T(8,128)(2,1)} fusion(bf16[512,2048]{1,0:T(8,128)(2,1)} %all-gather.4.cloned.1.call-done, bf16[512,8192]{1,0:T(8,128)(2,1)} %multiply_convert_fusion), kind=kOutput, calls=%fused_computation.10 | convolution fusion | flops 4299161600 | bytes 12582912 | tf_op jit(solution)/shard_map/dot_general | solution.py:70
  230.2 0.0 reduce-scatter.15.cloned.1.call-update
  230.2 0.3 reduce-scatter.13.cloned.1.call-start
  230.6 10.3 %convolution_convert_fusion.2 = bf16[2048,2048]{1,0:T(8,128)(2,1)} fusion(bf16[512,2048]{1,0:T(8,128)(2,1)} %all-gather.4.cloned.1.call-done, bf16[512,8192]{1,0:T(8,128)(2,1)} %multiply_convert_fusion), kind=kOutput, calls=%fused_computation.11 | convolution fusion | flops 4299161600 | bytes 12582912 | tf_op jit(solution)/shard_map/dot_general | solution.py:70
  240.8 0.0 reduce-scatter.13.cloned.1.call-update
  240.9 0.0 reduce-scatter.11.cloned.1.call-start
  240.9 10.1 %convolution_convert_fusion.3 = bf16[2048,2048]{1,0:T(8,128)(2,1)} fusion(bf16[512,2048]{1,0:T(8,128)(2,1)} %all-gather.4.cloned.1.call-done, bf16[512,8192]{1,0:T(8,128)(2,1)} %multiply_convert_fusion), kind=kOutput, calls=%fused_computation.12 | convolution fusion | flops 4299161600 | bytes 12582912 | tf_op jit(solution)/shard_map/dot_general | solution.py:70
  251.0 0.0 reduce-scatter.11.cloned.1.call-update
  251.0 0.6 dynamic_slice.3
  251.6 11.0 %reduce-scatter.9.cloned.1.call-done = f32[128,2048]{1,0:T(8,128)} async-done(((f32[512,2048]{1,0:T(8,128)}), f32[128,2048]{1,0:T(8,128)}) %reduce-scatter.9.cloned.1.call-update) | async-done | bytes 1048592 | tf_op jit(solution)/shard_map/reduce_scatter | solution.py:74
  262.6 0.0 copy-done.3
  262.6 1.9 multiply_reduce_fusion.1
  264.5 2.8 subtract_multiply_fusion
  267.3 87.0 %reduce-scatter.17.cloned.1.call-done = bf16[256,2048]{1,0:T(8,128)(2,1)} async-done(((bf16[2048,2048]{1,0:T(8,128)(2,1)}), bf16[256,2048]{1,0:T(8,128)(2,1)}) %reduce-scatter.17.cloned.1.call-update) | async-done | bytes 1048592 | tf_op jit(solution)/shard_map/reduce_scatter | solution.py:73
  354.3 90.2 %reduce-scatter.15.cloned.1.call-done = bf16[256,2048]{1,0:T(8,128)(2,1)} async-done(((bf16[2048,2048]{1,0:T(8,128)(2,1)}), bf16[256,2048]{1,0:T(8,128)(2,1)}) %reduce-scatter.15.cloned.1.call-update) | async-done | bytes 1048592 | tf_op jit(solution)/shard_map/reduce_scatter | solution.py:73
  444.5 90.2 %reduce-scatter.13.cloned.1.call-done = bf16[256,2048]{1,0:T(8,128)(2,1)} async-done(((bf16[2048,2048]{1,0:T(8,128)(2,1)}), bf16[256,2048]{1,0:T(8,128)(2,1)}) %reduce-scatter.13.cloned.1.call-update) | async-done | bytes 1048592 | tf_op jit(solution)/shard_map/reduce_scatter | solution.py:73
  534.7 90.3 %reduce-scatter.11.cloned.1.call-done = bf16[256,2048]{1,0:T(8,128)(2,1)} async-done(((bf16[2048,2048]{1,0:T(8,128)(2,1)}), bf16[256,2048]{1,0:T(8,128)(2,1)}) %reduce-scatter.11.cloned.1.call-update) | async-done | bytes 1048592 | tf_op jit(solution)/shard_map/reduce_scatter | solution.py:73
  625.0 5.3 maximum_convert_fusion
  (21 shorter events, 0.2 us)
Async XLA Ops:
  7.2 1.6 copy-start
  7.2 67.8 %copy-start.6 = (f32[2048]{0:T(1024)S(1)}, f32[2048]{0:T(1024)}, u32[]{:S(2)}) copy-start(f32[2048]{0:T(1024)} %param.12) | copy-start | bytes 24580
  7.2 67.8 %copy-start.4 = (bf16[128,2048]{1,0:T(8,128)(2,1)S(1)}, bf16[128,2048]{1,0:T(8,128)(2,1)}, u32[]{:S(2)}) copy-start(bf16[128,2048]{1,0:T(8,128)(2,1)} %param.11) | copy-start | bytes 1572868
  7.2 69.4 %copy-start.7 = (f32[2048]{0:T(1024)S(1)}, f32[2048]{0:T(1024)}, u32[]{:S(2)}) copy-start(f32[2048]{0:T(1024)} %param.13) | copy-start | bytes 24580
  7.2 66.4 %reduce-scatter.7.cloned.1.call-start = ((), (), s32[]{:S(2)}) async-start(), calls=%async_computation.6 | async-start | bytes 5242880 | tf_op jit(solution)/shard_map/reduce_scatter | solution.py:33
  18.1 61.4 %copy-start.8 = (f32[512,4]{0,1:T(4,128)S(1)}, f32[512,4]{0,1:T(4,128)}, u32[]{:S(2)}) copy-start(f32[512,4]{0,1:T(4,128)} %param.17) | copy-start | bytes 24580
  18.1 61.5 %copy-start.9 = (s32[512,4]{0,1:T(4,128)S(1)}, s32[512,4]{0,1:T(4,128)}, u32[]{:S(2)}) copy-start(s32[512,4]{0,1:T(4,128)} %param.16) | copy-start | bytes 24580
  18.1 96.2 %copy-start.5 = (f32[8192]{0:T(1024)S(1)}, f32[8192]{0:T(1024)}, u32[]{:S(2)}) copy-start(f32[8192]{0:T(1024)} %param.15) | copy-start | bytes 98308
  18.2 96.1 %all-gather.4.cloned.1.call-start = ((), (), s32[]{:S(2)}) async-start(), calls=%async_computation.7 | async-start | bytes 2621440 | tf_op jit(solution)/shard_map/all_gather | solution.py:42
  79.0 183.6 %reduce-scatter.9.cloned.1.call-start = ((), (), s32[]{:S(2)}) async-start(), calls=%async_computation.8 | async-start | bytes 5242880 | tf_op jit(solution)/shard_map/reduce_scatter | solution.py:74
  141.6 24.6 %copy-start.2 = (f32[512,8192]{1,0:T(8,128)S(1)}, f32[512,8192]{1,0:T(8,128)}, u32[]{:S(2)}) copy-start(f32[512,8192]{1,0:T(8,128)} %get-tuple-element.22) | copy-start | bytes 50331652
  209.9 144.4 %reduce-scatter.17.cloned.1.call-start = ((), (), s32[]{:S(2)}) async-start(), calls=%async_computation.12 | async-start | bytes 9437184 | tf_op jit(solution)/shard_map/reduce_scatter | solution.py:73
  220.2 224.3 %reduce-scatter.15.cloned.1.call-start = ((), (), s32[]{:S(2)}) async-start(), calls=%async_computation.11 | async-start | bytes 9437184 | tf_op jit(solution)/shard_map/reduce_scatter | solution.py:73
  230.2 304.4 %reduce-scatter.13.cloned.1.call-start = ((), (), s32[]{:S(2)}) async-start(), calls=%async_computation.10 | async-start | bytes 9437184 | tf_op jit(solution)/shard_map/reduce_scatter | solution.py:73
  240.9 384.1 %reduce-scatter.11.cloned.1.call-start = ((), (), s32[]{:S(2)}) async-start(), calls=%async_computation.9 | async-start | bytes 9437184 | tf_op jit(solution)/shard_map/reduce_scatter | solution.py:73
  251.0 11.6 %copy-start.3 = (f32[128,2048]{1,0:T(8,128)S(1)}, f32[128,2048]{1,0:T(8,128)}, u32[]{:S(2)}) copy-start(f32[128,2048]{1,0:T(8,128)} %reduce-scatter.7.cloned.1.call-done) | copy-start | bytes 3145732
  262.6 367.7 %copy-start.1 = (bf16[512,2048]{1,0:T(8,128)(2,1)S(1)}, bf16[512,2048]{1,0:T(8,128)(2,1)}, u32[]{:S(2)}) copy-start(bf16[512,2048]{1,0:T(8,128)(2,1)} %param.9) | copy-start | bytes 6291460
Sparse Core Ops, SparseCore 0:
  18.3 55.3 reduce-scatter.6
  79.1 35.1 all-gather.3
  210.0 52.5 reduce-scatter.8
  264.8 89.5 reduce-scatter.16
  356.5 87.9 reduce-scatter.14
  446.6 88.0 reduce-scatter.12
  537.0 87.9 reduce-scatter.10
